TPU v7x, 32 devices: a whole 2x2x4 slice. The times are simulated.
32 devices in a mesh: sp: 16 (over z, y, x), tp: 2 (over core).
Axes of the slice: x: 2, y: 2, z: 4, core: 2. Of those that a mesh axis runs over, the one named last changes fastest.
Arguments:
- resid: bfloat16 [6144, 2048], P('sp'), may hold values from -6 to 6
- x_branch: bfloat16 [6144, 2048], P('sp', 'tp'), may hold values from -6 to 6
- gate_branch: bfloat16 [6144, 2048], P('sp', 'tp'), may hold values from -6 to 6
- conv_w: float32 [4, 2048], P(None, 'tp'), may hold values from -3 to 3
- gate_a_w: bfloat16 [32, 64, 64], P('tp'), may hold values from -0.75 to 0.75
- gate_x_w: bfloat16 [32, 64, 64], P('tp'), may hold values from -0.75 to 0.75
- decay_rate: float32 [2048], P('tp'), may hold values from 0 to 0.01, as said below
- decay_extra: float32 [6144, 2048], P('sp', 'tp'), may hold values from -3 to 0, as said below
- w_proj: bfloat16 [2048, 2048], P('tp'), may hold values from -0.125 to 0.125
- mix_gain: float32 [2048], replicated, may hold values from 0.1 to 1.9
- pre_gain: float32 [2048], replicated, may hold values from 0.1 to 1.9
- w_gate: bfloat16 [2048, 5632], P('sp', 'tp'), may hold values from -0.125 to 0.125
- w_up: bfloat16 [2048, 5632], P('sp', 'tp'), may hold values from -0.125 to 0.125
- w_down: bfloat16 [5632, 2048], P('tp', 'sp'), may hold values from -0.078125 to 0.078125
- out_gain: float32 [2048], replicated, may hold values from 0.1 to 1.9
Outputs:
- stream_out: bfloat16 [6144, 2048], P(('sp', 'tp'))
Inputs may be any that keep to these rules, and one draw needn't show every extreme that they name: `decay_rate`: positive rates. `decay_extra`: non-positive values.
All inputs are finite; a program needn't handle non-finite values.
Results may differ from a plain program's by a relative error of at most 0.015.
Values may be sent and summed in bfloat16 or wider, within the bound.
A program may use at most 128 MiB of HBM per device.

v0:
```python
import jax
import jax.numpy as jnp
from jax import lax
from jax.sharding import PartitionSpec as P

LRU_SCALE = 8.0
NORM_EPS = 1e-06


def from_behind(value, axis, steps):
    count = lax.axis_size(axis)
    first, last = (max(0, -steps), min(count, count - steps))
    return lax.ppermute(value, axis, [(source, source + steps) for source in range(first, last)])


def prefix(part, axis, combine, identity):
    place = lax.axis_index(axis)
    gathered = jax.tree.map(lambda a: lax.all_gather(a, axis), part)
    state = jax.tree.map(lambda a, e: jnp.zeros_like(a) + jnp.asarray(e, a.dtype), part, identity)

    def one(turn, state):
        return combine(
            state, jax.tree.map(lambda a: lax.dynamic_index_in_dim(a, turn, 0, False), gathered)
        )

    return lax.fori_loop(0, place, one, state)


def chain(earlier, later):
    return (earlier[0] * later[0], later[0] * earlier[1] + later[1])


def rms_scale(values, gains):
    return values * lax.rsqrt(jnp.mean(values * values, axis=-1, keepdims=True) + NORM_EPS) * gains


def shards(
    resid,
    x_branch,
    gate_branch,
    conv_w,
    gate_a_w,
    gate_x_w,
    decay_rate,
    decay_extra,
    w_proj,
    mix_gain,
    pre_gain,
    w_gate,
    w_up,
    w_down,
    out_gain,
):
    length = x_branch.shape[0]
    width = x_branch.shape[1]
    taps = conv_w.shape[0]
    before = from_behind(x_branch[length - (taps - 1) :], "sp", 1)
    padded = jnp.concatenate([before, x_branch], axis=0).astype(jnp.float32)
    conv = padded[0:length] * conv_w[0]
    for tap in range(1, taps):
        conv = conv + padded[tap : tap + length] * conv_w[tap]
    conv_out = conv.astype(jnp.bfloat16)
    nblocks = gate_a_w.shape[0]
    grouped = conv_out.reshape(length, nblocks, gate_a_w.shape[1])
    recur = jax.nn.sigmoid(
        jnp.einsum("rnc,ncd->rnd", grouped, gate_a_w, preferred_element_type=jnp.float32).reshape(
            length, width
        )
    )
    inject = jax.nn.sigmoid(
        jnp.einsum("rnc,ncd->rnd", grouped, gate_x_w, preferred_element_type=jnp.float32).reshape(
            length, width
        )
    )
    log_decay = -LRU_SCALE * recur * decay_rate + decay_extra
    decay = jnp.exp(log_decay)
    drive = jnp.sqrt(-jnp.expm1(2.0 * log_decay)) * inject * conv_out.astype(jnp.float32)
    prod_local, state_local = lax.associative_scan(chain, (decay, drive), axis=0)
    identity = (jnp.ones((width,), jnp.float32), jnp.zeros((width,), jnp.float32))
    carried = prefix((prod_local[-1], state_local[-1]), "sp", chain, identity)
    state = state_local + prod_local * carried[1][None, :]
    mixer = (state * jax.nn.gelu(gate_branch.astype(jnp.float32))).astype(jnp.bfloat16)
    share_rows = length // lax.axis_size("tp")
    first = lax.axis_index("tp") * share_rows
    mixed = lax.psum(
        jnp.dot(mixer, w_proj, preferred_element_type=jnp.float32).astype(jnp.bfloat16), "tp"
    ).astype(jnp.float32)
    stream = resid.astype(jnp.float32) + rms_scale(mixed, mix_gain)
    normed = rms_scale(stream, pre_gain).astype(jnp.bfloat16)
    after_mix = lax.dynamic_slice_in_dim(stream, first, share_rows, 0)
    gate_full, up_full = (
        lax.all_gather(w_gate, "sp", axis=0, tiled=True),
        lax.all_gather(w_up, "sp", axis=0, tiled=True),
    )
    down_full = lax.all_gather(w_down, "sp", axis=1, tiled=True)
    gate = jnp.dot(normed, gate_full, preferred_element_type=jnp.float32)
    upward = jnp.dot(normed, up_full, preferred_element_type=jnp.float32)
    hidden = (jax.nn.silu(gate) * upward).astype(jnp.bfloat16)
    ffn = lax.psum_scatter(
        jnp.dot(hidden, down_full, preferred_element_type=jnp.float32).astype(jnp.bfloat16),
        "tp",
        scatter_dimension=0,
        tiled=True,
    ).astype(jnp.float32)
    return (after_mix + 0.5 * rms_scale(ffn, out_gain)).astype(jnp.bfloat16)


def solution(mesh):
    return jax.shard_map(
        shards,
        mesh=mesh,
        in_specs=(
            P("sp", None),
            P("sp", "tp"),
            P("sp", "tp"),
            P(None, "tp"),
            P("tp", None, None),
            P("tp", None, None),
            P("tp"),
            P("sp", "tp"),
            P("tp", None),
            P(),
            P(),
            P("sp", "tp"),
            P("sp", "tp"),
            P("tp", "sp"),
            P(),
        ),
        out_specs=P(("sp", "tp"), None),
        check_vma=False,
    )
```

profile of v0, /device:TPU:0, one launch (start us, length us, event | category | flops | bytes accessed | tf_op | source)
XLA Modules:
  0.0 737.7 jit_solution(13793167642620603508)
XLA Ops:
  8.1 4.9 collective-permute-start
  14.6 1.4 maximum_convert_fusion
  17.8 1.8 add_divide_fusion.1
  19.6 1.7 copy.106
  21.3 1.8 add_divide_fusion
  23.0 1.6 copy.108
  24.6 5.3 convert_multiply_fusion.7
  30.0 4.5 slice.281
  34.4 2.1 slice.282
  36.6 2.1 slice.280
  38.7 2.2 slice.284
  40.9 3.4 multiply_add_fusion.2
  44.2 2.7 slice.287
  46.9 2.7 slice.288
  49.6 2.7 slice.286
  52.4 2.7 slice.290
  55.1 2.4 multiply_add_fusion.3
  57.4 1.7 slice.293
  59.1 1.7 slice.294
  60.8 1.7 slice.292
  62.5 1.7 slice.296
  64.1 2.0 multiply_add_fusion.4
  67.4 1.6 slice.298
  69.0 1.6 slice.302
  70.6 1.7 multiply_add_fusion.5
  73.6 1.5 slice.304
  75.1 1.5 slice.308
  76.6 1.6 multiply_add_fusion.6
  79.4 1.5 slice.310
  80.9 1.5 slice.314
  82.3 1.4 multiply_add_fusion.7
  84.5 1.4 slice.318
  87.8 1.4 slice.326
  89.1 1.3 slice.366
  94.5 1.5 slice.303
  96.6 1.4 slice.390
  102.2 1.7 slice.291
  103.9 1.7 slice.334
  106.9 1.4 slice.362
  108.2 2.7 slice.285
  111.0 2.8 slice.336
  113.8 1.4 slice.361
  115.1 1.4 slice.387
  116.5 2.3 slice.279
  118.8 2.2 slice.338
  128.0 3.1 pad.113
  134.1 1.4 fusion.21
  135.6 3.2 pad.112
  139.6 42.0 %all-gather.1 = f32[16,1,1024]{2,1,0:T(1,128)S(1)} all-gather(f32[1,1,1024]{2,1,0:T(1,128)S(1)} %add_bitcast_fusion), channel_id=1, replica_groups=mesh['sp'=16,'tp'=2] {'sp'}, dimensions={0}, use_global_device_ids=true | all-gather | bytes 69632 | tf_op jit(solution)/shard_map/all_gather | solution.py:18
  181.7 3.1 pad.129
  184.9 3.2 pad.128
  188.9 35.8 %all-gather = f32[16,1,1024]{2,1,0:T(1,128)S(1)} all-gather(f32[1,1,1024]{2,1,0:T(1,128)S(1)} %add_bitcast_fusion.1), channel_id=1, replica_groups=mesh['sp'=16,'tp'=2] {'sp'}, dimensions={0}, use_global_device_ids=true | all-gather | bytes 69632 | tf_op jit(solution)/shard_map/all_gather | solution.py:18
  224.7 7.0 convolution_convert_fusion.1
  233.6 17.4 %all-reduce.34.cloned.1.call-done = bf16[384,2048]{1,0:T(8,128)(2,1)} async-done(((bf16[384,2048]{1,0:T(8,128)(2,1)}), bf16[384,2048]{1,0:T(8,128)(2,1)}) %all-reduce.34.cloned.1.call-update) | async-done | bytes 1572880 | tf_op jit(solution)/shard_map/psum | solution.py:85
  250.9 1.9 fusion.1
  252.9 2.3 multiply_reduce_fusion
  255.2 119.6 %all-gather.6.cloned.1.call-done = bf16[2048,2816]{1,0:T(8,128)(2,1)} async-done(((bf16[128,2816]{1,0:T(8,128)(2,1)}), bf16[2048,2816]{1,0:T(8,128)(2,1)}) %all-gather.6.cloned.1.call-update) | async-done | bytes 11534352 | tf_op jit(solution)/shard_map/all_gather | solution.py:92
  374.9 9.6 %fusion.43 = f32[384,2816]{1,0:T(8,128)} fusion(bf16[2048,2816]{1,0:T(8,128)(2,1)} %all-gather.6.cloned.1.call-done, f32[384,2048]{1,0:T(8,128)S(1)} %get-tuple-element.61, f32[2048]{0:T(1024)S(1)} %copy-done.38, f32[384]{0:T(512)S(1)} %add_rsqrt_fusion), kind=kOutput, calls=%fused_computation.118 | convolution fusion | flops 4431544320 | bytes 19015168 | tf_op jit(solution)/shard_map/dot_general | solution.py:96
  384.4 173.1 %all-gather.10.cloned.1.call-done = bf16[2816,2048]{1,0:T(8,128)(2,1)} async-done(((bf16[2816,128]{1,0:T(8,128)(2,1)}), bf16[2816,2048]{1,0:T(8,128)(2,1)}) %all-gather.10.cloned.1.call-update) | async-done | bytes 11534352 | tf_op jit(solution)/shard_map/all_gather | solution.py:95
  557.5 142.0 %all-gather.8.cloned.1.call-done = bf16[2048,2816]{1,0:T(8,128)(2,1)} async-done(((bf16[128,2816]{1,0:T(8,128)(2,1)}), bf16[2048,2816]{1,0:T(8,128)(2,1)}) %all-gather.8.cloned.1.call-update) | async-done | bytes 11534352 | tf_op jit(solution)/shard_map/all_gather | solution.py:93
  699.5 19.3 %convolution_convert_fusion = bf16[384,2048]{1,0:T(8,128)(2,1)} fusion(bf16[2816,2048]{1,0:T(8,128)(2,1)} %all-gather.10.cloned.1.call-done, bf16[2048,2816]{1,0:T(8,128)(2,1)} %all-gather.8.cloned.1.call-done, f32[384,2816]{1,0:T(8,128)} %fusion.43, f32[384,2048]{1,0:T(8,128)S(1)} %get-tuple-element.61, f32[2048]{0:T(1024)S(1)} %copy-done.38, ...), kind=kOutput, calls=%fused_computation.12 | convolution fusion | flops 8868003840 | bytes 32122368 | tf_op jit(solution)/shard_map/dot_general | solution.py:100
  718.9 7.4 reduce-scatter.2.cloned.1.call-done
  726.3 1.4 fusion.4
  727.7 2.4 fusion.8
  (189 shorter events, 33.9 us)
Async XLA Ops:
  7.4 10.4 %copy-start = (bf16[16,64,64]{2,1,0:T(8,128)(2,1)S(1)}, bf16[16,64,64]{2,1,0:T(8,128)(2,1)}, u32[]{:S(2)}) copy-start(bf16[16,64,64]{2,1,0:T(8,128)(2,1)} %param.21) | copy-start | bytes 393220
  7.4 243.6 %all-reduce.34.cloned.1.call-start = ((), (), s32[]{:S(2)}) async-start(), calls=%async_computation.1 | async-start | bytes 3145728 | tf_op jit(solution)/shard_map/psum | solution.py:85
  8.1 6.5 collective-permute-start
  19.6 1.7 copy-start.37
  29.9 4.5 copy-start.2
  116.5 5.7 copy-start.15
  116.5 5.7 copy-start.16
  116.5 5.7 copy-start.17
  116.5 6.0 copy-start.18
  116.5 6.0 copy-start.19
  116.5 6.0 copy-start.26
  116.5 6.0 copy-start.27
  118.8 3.8 copy-start.14
  118.8 3.9 copy-start.33
  118.8 3.9 copy-start.32
  121.6 2.1 copy-start.31
  122.2 1.6 copy-start.30
  122.6 1.3 copy-start.13
  122.8 1.2 copy-start.29
  123.7 0.7 copy-start.28
  124.0 0.9 copy-start.11
  124.0 1.0 copy-start.12
  124.5 0.7 copy-start.25
  125.0 0.7 copy-start.24
  125.7 1.0 copy-start.9
  125.7 1.2 copy-start.10
  126.9 0.7 copy-start.23
  128.0 3.1 copy-start.22
  132.5 1.4 copy-start.4
  132.5 1.6 copy-start.5
  134.1 1.4 copy-start.21
  135.6 3.2 copy-start.8
  135.6 46.1 %copy-start.7 = (f32[192,1024]{1,0:T(8,128)S(1)}, f32[192,1024]{1,0:T(8,128)}, u32[]{:S(2)}) copy-start(f32[192,1024]{1,0:T(8,128)} %add.291) | copy-start | bytes 2359300
  138.8 46.0 %copy-start.6 = (f32[191,1024]{1,0:T(8,128)S(1)}, f32[191,1024]{1,0:T(8,128)}, u32[]{:S(2)}) copy-start(f32[191,1024]{1,0:T(8,128)} %get-tuple-element.71) | copy-start | bytes 2347012
  138.8 46.0 %copy-start.20 = (f32[1,1024]{1,0:T(1,128)S(1)}, f32[1,1024]{1,0:T(1,128)}, u32[]{:S(2)}) copy-start(f32[1,1024]{1,0:T(1,128)} %slice.386) | copy-start | bytes 12292
  184.9 39.8 %copy-start.36 = (bf16[384,1024]{1,0:T(8,128)(2,1)S(1)}, bf16[384,1024]{1,0:T(8,128)(2,1)}, u32[]{:S(2)}) copy-start(bf16[384,1024]{1,0:T(8,128)(2,1)} %param.19) | copy-start | bytes 2359300
  231.8 143.1 %all-gather.6.cloned.1.call-start = ((), (), s32[]{:S(2)}) async-start(), calls=%async_computation.2 | async-start | bytes 12255232 | tf_op jit(solution)/shard_map/all_gather | solution.py:92
  232.3 20.5 %copy-start.34 = (f32[2048]{0:T(1024)S(1)}, f32[2048]{0:T(1024)}, u32[]{:S(2)}) copy-start(f32[2048]{0:T(1024)} %param.26) | copy-start | bytes 24580
  232.3 325.2 %all-gather.10.cloned.1.call-start = ((), (), s32[]{:S(2)}) async-start(), calls=%async_computation.4 | async-start | bytes 12255232 | tf_op jit(solution)/shard_map/all_gather | solution.py:95
  232.9 466.6 %all-gather.8.cloned.1.call-start = ((), (), s32[]{:S(2)}) async-start(), calls=%async_computation.3 | async-start | bytes 12255232 | tf_op jit(solution)/shard_map/all_gather | solution.py:93
  233.5 492.8 %reduce-scatter.2.cloned.1.call-start = ((), (), s32[]{:S(2)}) async-start(), calls=%async_computation.5 | async-start | bytes 2359296 | tf_op jit(solution)/shard_map/reduce_scatter | solution.py:99
  250.9 1.9 copy-start.3
  252.9 122.0 %copy-start.38 = (f32[2048]{0:T(1024)S(1)}, f32[2048]{0:T(1024)}, u32[]{:S(2)}) copy-start(f32[2048]{0:T(1024)} %param.27) | copy-start | bytes 24580
  718.9 8.8 %copy-start.35 = (f32[2048]{0:T(1024)S(1)}, f32[2048]{0:T(1024)}, u32[]{:S(2)}) copy-start(f32[2048]{0:T(1024)} %param.31) | copy-start | bytes 24580
  727.7 2.4 copy-start.1
Sparse Core Ops, SparseCore 0:
  231.9 19.0 all-reduce.33
  719.0 7.2 reduce-scatter.1
Sparse Core Ops, SparseCore 1:
  235.0 139.8 all-gather.5
  377.4 180.0 all-gather.9
  560.1 139.3 all-gather.7
where the time goes:
time: 740 us; the launch traced here: 738 us
  waiting for transfers between devices  461 us (62%)
  local copies, waits for them, and re-layouts  103 us (14%)
  blocking collectives  77.8 us (11%)
  matrix products  39.4 us (5%)
  other arithmetic  35.2 us (5%)
  between operations  15.9 us (2%)
    all_gather x1, waiting for transfers between devices, shards(): down_full = lax.all_gather(w_down, 'sp', axis=1, tiled=True)  173 us
    all_gather x1, waiting for transfers between devices, shards(): lax.all_gather(w_up, 'sp', axis=0, tiled=True)  142 us
    all_gather x1, waiting for transfers between devices, shards(): lax.all_gather(w_gate, 'sp', axis=0, tiled=True)  120 us
    slice x56, local copies, waits for them, and re-layouts, shards(): lax.associative_scan(chain, (decay, drive), axis=0)  79.8 us
    all_gather x2, blocking collectives, prefix(): gathered = jax.tree.map(lambda a: lax.all_gather(a, axis), part)  77.8 us
    dot_general x1, matrix products, shards(): jnp.dot(hidden, down_full, preferred_element_type=jnp.float32)  19.3 us
    psum x1, waiting for transfers between devices, shards(): lax.psum(jnp.dot(mixer, w_proj, preferred_element_type=jnp.float32).astyp...  17.4 us
    add x15, other arithmetic, chain(): return (earlier[0] * later[0], later[0] * earlier[1] + later[1])  15 us
  transfers between devices with their start and end apart: 6, of which 5 were waited for; matrix products, arithmetic and copies ran while one was open for 2% of the time, Pallas kernels for 0%

commit v1 on v0

--- a/solution.py
+++ b/solution.py
@@ -92,7 +92,12 @@
         lax.all_gather(w_gate, "sp", axis=0, tiled=True),
         lax.all_gather(w_up, "sp", axis=0, tiled=True),
     )
-    down_full = lax.all_gather(w_down, "sp", axis=1, tiled=True)
+    ring = [w_down]
+    for hop in range(15):
+        ring.append(lax.ppermute(ring[-1], "sp", [(dev, (dev + 1) % 16) for dev in range(16)]))
+    down_full = jnp.roll(
+        jnp.concatenate(ring[::-1], axis=1), (lax.axis_index("sp") + 1) * ring[0].shape[1], axis=1
+    )
     gate = jnp.dot(normed, gate_full, preferred_element_type=jnp.float32)
     upward = jnp.dot(normed, up_full, preferred_element_type=jnp.float32)
     hidden = (jax.nn.silu(gate) * upward).astype(jnp.bfloat16)

time: 740 us -> 783 us (1.058)
  local copies, waits for them, and re-layouts: 103 us -> 140 us
  other arithmetic: 35.2 us -> 45.1 us
    ppermute x0 -> x15, waiting for transfers between devices: none -> 449 us  [shards(): lax.ppermute(ring[-1], 'sp', [(dev, (dev + 1) % 16) for dev in range(16)])]
    all_gather x1 -> x0, waiting for transfers between devices: 173 us -> none  [shards(): down_full = lax.all_gather(w_down, 'sp', axis=1, tiled=True)]
    all_gather x1, waiting for transfers between devices: 142 us -> 0.01 us  [shards(): lax.all_gather(w_up, 'sp', axis=0, tiled=True)]
    all_gather x1, waiting for transfers between devices: 120 us -> 0.01 us  [shards(): lax.all_gather(w_gate, 'sp', axis=0, tiled=True)]
    unnamed x80 -> x147, local copies, waits for them, and re-layouts: 2.7 us -> 41.7 us
    psum x1, waiting for transfers between devices: 17.4 us -> 0.01 us  [shards(): lax.psum(jnp.dot(mixer, w_proj, preferred_element_type=jnp.float32).astyp...]
  transfers between devices with their start and end apart: 6 -> 20, of which waited for: 5 -> 16; matrix products, arithmetic and copies ran while one was open for 2% -> 6% of each run, Pallas kernels for 0% -> 0%
where the time goes in v1:
time: 783 us; the launch traced here: 780 us
  waiting for transfers between devices  455 us (58%)
  local copies, waits for them, and re-layouts  140 us (18%)
  blocking collectives  77.8 us (10%)
  other arithmetic  45.1 us (6%)
  matrix products  39.9 us (5%)
  between operations  15.6 us (2%)
    ppermute x15, waiting for transfers between devices, shards(): lax.ppermute(ring[-1], 'sp', [(dev, (dev + 1) % 16) for dev in range(16)])  449 us
    slice x56, local copies, waits for them, and re-layouts, shards(): lax.associative_scan(chain, (decay, drive), axis=0)  78 us
    all_gather x2, blocking collectives, prefix(): gathered = jax.tree.map(lambda a: lax.all_gather(a, axis), part)  77.8 us
    unnamed x147, local copies, waits for them, and re-layouts  41.7 us
    dot_general x1, matrix products, shards(): jnp.dot(hidden, down_full, preferred_element_type=jnp.float32)  19.3 us
    add x15, other arithmetic, chain(): return (earlier[0] * later[0], later[0] * earlier[1] + later[1])  18 us
  transfers between devices with their start and end apart: 20, of which 16 were waited for; matrix products, arithmetic and copies ran while one was open for 6% of the time, Pallas kernels for 0%

profile of v1, /device:TPU:0, one launch (start us, length us, event | category | flops | bytes accessed | tf_op | source)
XLA Modules:
  0.0 780.1 jit_solution(17684429321763095183)
XLA Ops:
  8.1 4.9 collective-permute-start
  17.8 1.8 add_divide_fusion
  19.6 1.6 copy.108
  21.2 1.8 add_divide_fusion.1
  23.0 1.6 copy.106
  24.6 5.3 convert_multiply_fusion.7
  29.9 2.2 slice.338
  32.2 2.1 slice.282
  34.3 2.2 slice.279
  36.5 2.1 slice.280
  38.7 2.2 slice.281
  40.8 2.1 slice.284
  43.0 3.4 multiply_add_fusion.2
  46.4 2.7 slice.288
  49.1 2.7 slice.287
  51.8 2.7 slice.286
  54.5 2.7 slice.290
  57.2 2.4 multiply_add_fusion.3
  59.5 1.7 slice.334
  61.3 1.7 slice.294
  62.9 1.7 slice.291
  64.6 1.7 slice.292
  66.3 1.7 slice.293
  68.0 1.7 slice.296
  69.7 1.9 multiply_add_fusion.4
  72.9 1.6 slice.298
  74.5 1.6 slice.302
  76.1 1.7 multiply_add_fusion.5
  77.8 1.5 slice.330
  79.3 1.5 slice.306
  84.3 1.6 multiply_add_fusion.6
  104.2 1.6 slice.297
  109.6 2.7 slice.336
  112.4 2.7 slice.285
  138.9 3.1 pad.128
  142.0 3.2 pad.129
  145.4 3.1 pad.112
  149.6 41.8 %all-gather = f32[16,1,1024]{2,1,0:T(1,128)S(1)} all-gather(f32[1,1,1024]{2,1,0:T(1,128)S(1)} %add_bitcast_fusion.1), channel_id=1, replica_groups=mesh['sp'=16,'tp'=2] {'sp'}, dimensions={0}, use_global_device_ids=true | all-gather | bytes 69632 | tf_op jit(solution)/shard_map/all_gather | solution.py:18
  192.2 35.9 %all-gather.1 = f32[16,1,1024]{2,1,0:T(1,128)S(1)} all-gather(f32[1,1,1024]{2,1,0:T(1,128)S(1)} %add_bitcast_fusion), channel_id=1, replica_groups=mesh['sp'=16,'tp'=2] {'sp'}, dimensions={0}, use_global_device_ids=true | all-gather | bytes 69632 | tf_op jit(solution)/shard_map/all_gather | solution.py:18
  228.4 7.5 convolution_convert_fusion
  236.6 2.1 collective-permute-start.1
  238.7 24.5 %collective-permute-done.1 = bf16[2816,128]{1,0:T(8,128)(2,1)S(1)} collective-permute-done((bf16[2816,128]{1,0:T(8,128)(2,1)S(1)}, bf16[2816,128]{1,0:T(8,128)(2,1)S(1)}, u32[]{:S(2)}, u32[]{:S(2)}) %collective-permute-start.1) | collective-permute-done | bytes 720928 | tf_op jit(solution)/shard_map/ppermute | solution.py:97
  264.1 24.5 %collective-permute-done.2 = bf16[2816,128]{1,0:T(8,128)(2,1)S(1)} collective-permute-done((bf16[2816,128]{1,0:T(8,128)(2,1)S(1)}, bf16[2816,128]{1,0:T(8,128)(2,1)S(1)}, u32[]{:S(2)}, u32[]{:S(2)}) %collective-permute-start.2) | collective-permute-done | bytes 720928 | tf_op jit(solution)/shard_map/ppermute | solution.py:97
  288.7 36.2 %collective-permute-done.3 = bf16[2816,128]{1,0:T(8,128)(2,1)S(1)} collective-permute-done((bf16[2816,128]{1,0:T(8,128)(2,1)S(1)}, bf16[2816,128]{1,0:T(8,128)(2,1)S(1)}, u32[]{:S(2)}, u32[]{:S(2)}) %collective-permute-start.3) | collective-permute-done | bytes 720928 | tf_op jit(solution)/shard_map/ppermute | solution.py:97
  324.9 26.7 %collective-permute-done.4 = bf16[2816,128]{1,0:T(8,128)(2,1)S(1)} collective-permute-done((bf16[2816,128]{1,0:T(8,128)(2,1)S(1)}, bf16[2816,128]{1,0:T(8,128)(2,1)S(1)}, u32[]{:S(2)}, u32[]{:S(2)}) %collective-permute-start.4) | collective-permute-done | bytes 720928 | tf_op jit(solution)/shard_map/ppermute | solution.py:97
  352.5 37.5 %collective-permute-done.5 = bf16[2816,128]{1,0:T(8,128)(2,1)S(1)} collective-permute-done((bf16[2816,128]{1,0:T(8,128)(2,1)S(1)}, bf16[2816,128]{1,0:T(8,128)(2,1)S(1)}, u32[]{:S(2)}, u32[]{:S(2)}) %collective-permute-start.5) | collective-permute-done | bytes 720928 | tf_op jit(solution)/shard_map/ppermute | solution.py:97
  390.8 34.3 %collective-permute-done.6 = bf16[2816,128]{1,0:T(8,128)(2,1)S(1)} collective-permute-done((bf16[2816,128]{1,0:T(8,128)(2,1)S(1)}, bf16[2816,128]{1,0:T(8,128)(2,1)S(1)}, u32[]{:S(2)}, u32[]{:S(2)}) %collective-permute-start.6) | collective-permute-done | bytes 720928 | tf_op jit(solution)/shard_map/ppermute | solution.py:97
  426.0 36.8 %collective-permute-done.7 = bf16[2816,128]{1,0:T(8,128)(2,1)S(1)} collective-permute-done((bf16[2816,128]{1,0:T(8,128)(2,1)S(1)}, bf16[2816,128]{1,0:T(8,128)(2,1)S(1)}, u32[]{:S(2)}, u32[]{:S(2)}) %collective-permute-start.7) | collective-permute-done | bytes 720928 | tf_op jit(solution)/shard_map/ppermute | solution.py:97
  463.6 29.2 %collective-permute-done.8 = bf16[2816,128]{1,0:T(8,128)(2,1)S(1)} collective-permute-done((bf16[2816,128]{1,0:T(8,128)(2,1)S(1)}, bf16[2816,128]{1,0:T(8,128)(2,1)S(1)}, u32[]{:S(2)}, u32[]{:S(2)}) %collective-permute-start.8) | collective-permute-done | bytes 720928 | tf_op jit(solution)/shard_map/ppermute | solution.py:97
  493.7 25.1 %collective-permute-done.9 = bf16[2816,128]{1,0:T(8,128)(2,1)S(1)} collective-permute-done((bf16[2816,128]{1,0:T(8,128)(2,1)S(1)}, bf16[2816,128]{1,0:T(8,128)(2,1)S(1)}, u32[]{:S(2)}, u32[]{:S(2)}) %collective-permute-start.9) | collective-permute-done | bytes 720928 | tf_op jit(solution)/shard_map/ppermute | solution.py:97
  519.7 33.7 %collective-permute-done.10 = bf16[2816,128]{1,0:T(8,128)(2,1)S(1)} collective-permute-done((bf16[2816,128]{1,0:T(8,128)(2,1)S(1)}, bf16[2816,128]{1,0:T(8,128)(2,1)S(1)}, u32[]{:S(2)}, u32[]{:S(2)}) %collective-permute-start.10) | collective-permute-done | bytes 720928 | tf_op jit(solution)/shard_map/ppermute | solution.py:97
  554.2 23.1 %collective-permute-done.11 = bf16[2816,128]{1,0:T(8,128)(2,1)S(1)} collective-permute-done((bf16[2816,128]{1,0:T(8,128)(2,1)S(1)}, bf16[2816,128]{1,0:T(8,128)(2,1)S(1)}, u32[]{:S(2)}, u32[]{:S(2)}) %collective-permute-start.11) | collective-permute-done | bytes 720928 | tf_op jit(solution)/shard_map/ppermute | solution.py:97
  578.2 37.2 %collective-permute-done.12 = bf16[2816,128]{1,0:T(8,128)(2,1)S(1)} collective-permute-done((bf16[2816,128]{1,0:T(8,128)(2,1)S(1)}, bf16[2816,128]{1,0:T(8,128)(2,1)S(1)}, u32[]{:S(2)}, u32[]{:S(2)}) %collective-permute-start.12) | collective-permute-done | bytes 720928 | tf_op jit(solution)/shard_map/ppermute | solution.py:97
  616.3 33.1 %collective-permute-done.13 = bf16[2816,128]{1,0:T(8,128)(2,1)S(1)} collective-permute-done((bf16[2816,128]{1,0:T(8,128)(2,1)S(1)}, bf16[2816,128]{1,0:T(8,128)(2,1)S(1)}, u32[]{:S(2)}, u32[]{:S(2)}) %collective-permute-start.13) | collective-permute-done | bytes 720928 | tf_op jit(solution)/shard_map/ppermute | solution.py:97
  649.4 2.1 fusion.3
  651.5 34.9 %collective-permute-done.14 = bf16[2816,128]{1,0:T(8,128)(2,1)} collective-permute-done((bf16[2816,128]{1,0:T(8,128)(2,1)S(1)}, bf16[2816,128]{1,0:T(8,128)(2,1)}, u32[]{:S(2)}, u32[]{:S(2)}) %collective-permute-start.14) | collective-permute-done | bytes 720928 | tf_op jit(solution)/shard_map/ppermute | solution.py:97
  686.5 2.8 multiply_reduce_fusion
  689.3 12.2 %collective-permute-done.15 = bf16[2816,128]{1,0:T(8,128)(2,1)S(1)} collective-permute-done((bf16[2816,128]{1,0:T(8,128)(2,1)}, bf16[2816,128]{1,0:T(8,128)(2,1)S(1)}, u32[]{:S(2)}, u32[]{:S(2)}) %collective-permute-start.15) | collective-permute-done | bytes 720928 | tf_op jit(solution)/shard_map/ppermute | solution.py:97
  702.5 2.1 constant_dynamic-update-slice_fusion.30
  719.2 2.1 constant_dynamic-update-slice_fusion.14
  734.9 9.5 %fusion.49 = f32[384,2816]{1,0:T(8,128)} fusion(bf16[2048,2816]{1,0:T(8,128)(2,1)} %all-gather.5.cloned.1.call-done, f32[384,2048]{1,0:T(8,128)S(1)} %get-tuple-element.61, f32[2048]{0:T(1024)S(1)} %copy-done.56, f32[384]{0:T(512)S(1)} %add_rsqrt_fusion), kind=kOutput, calls=%fused_computation.153 | convolution fusion | flops 4431544320 | bytes 19015168 | tf_op jit(solution)/shard_map/dot_general | solution.py:101
  744.4 19.3 %fusion.6 = bf16[384,2048]{1,0:T(8,128)(2,1)} fusion(bf16[2816,4096]{1,0:T(8,128)(2,1)} %constant_dynamic-update-slice_fusion, s32[]{:T(128)S(6)} %select_n.24, bf16[2048,2816]{1,0:T(8,128)(2,1)} %all-gather.7.cloned.1.call-done, f32[384,2816]{1,0:T(8,128)} %fusion.49, f32[384,2048]{1,0:T(8,128)S(1)} %get-tuple-element.61, f32[2048]{0:T(1024)S(1)} %copy-done.56, ...), kind=kOutput, calls=%fused_computation.14 | convolution fusion | flops 8868003840 | bytes 32122372 | tf_op jit(solution)/shard_map/dot_general | solution.py:105
  763.8 5.1 reduce-scatter.2.cloned.1.call-done
  770.3 2.4 fusion.13
  (284 shorter events, 97.9 us)
Async XLA Ops:
  7.4 10.4 %copy-start = (bf16[16,64,64]{2,1,0:T(8,128)(2,1)S(1)}, bf16[16,64,64]{2,1,0:T(8,128)(2,1)}, u32[]{:S(2)}) copy-start(bf16[16,64,64]{2,1,0:T(8,128)(2,1)} %param.22) | copy-start | bytes 393220
  7.4 642.1 %all-reduce.34.cloned.1.call-start = ((), (), s32[]{:S(2)}) async-start(), calls=%async_computation.1 | async-start | bytes 3145728 | tf_op jit(solution)/shard_map/psum | solution.py:85
  8.1 6.5 collective-permute-start
  19.6 1.6 copy-start.55
  29.9 4.4 copy-start.2
  106.4 20.6 %copy-start.43 = (f32[23,1024]{1,0:T(8,128)S(1)}, f32[23,1024]{1,0:T(8,128)}, u32[]{:S(2)}) copy-start(f32[23,1024]{1,0:T(8,128)} %slice.332) | copy-start | bytes 282628
  119.8 7.2 copy-start.51
  119.8 7.2 copy-start.44
  124.3 4.9 copy-start.40
  124.4 4.9 copy-start.41
  126.8 2.6 copy-start.50
  129.4 1.8 copy-start.37
  129.4 1.8 copy-start.38
  130.3 1.9 copy-start.48
  131.2 2.3 copy-start.47
  135.5 2.0 copy-start.3
  135.5 2.0 copy-start.4
  137.4 1.4 copy-start.46
  138.8 3.2 copy-start.7
  138.8 6.4 copy-start.5
  138.8 6.4 copy-start.45
  142.0 6.5 copy-start.6
  145.4 83.0 %copy-start.54 = (bf16[384,1024]{1,0:T(8,128)(2,1)S(1)}, bf16[384,1024]{1,0:T(8,128)(2,1)}, u32[]{:S(2)}) copy-start(bf16[384,1024]{1,0:T(8,128)(2,1)} %param.19) | copy-start | bytes 2359300
  148.7 79.6 %copy-start.36 = (f32[384,1024]{1,0:T(8,128)}, f32[384,1024]{1,0:T(8,128)S(1)}, u32[]{:S(2)}) copy-start(f32[384,1024]{1,0:T(8,128)S(1)} %pad.113) | copy-start | bytes 4718596
  228.4 8.2 %copy-start.8 = (bf16[2816,128]{1,0:T(8,128)(2,1)S(1)}, bf16[2816,128]{1,0:T(8,128)(2,1)}, u32[]{:S(2)}) copy-start(bf16[2816,128]{1,0:T(8,128)(2,1)} %param.30) | copy-start | bytes 2162692
  235.9 450.5 %copy-start.52 = (f32[2048]{0:T(1024)S(1)}, f32[2048]{0:T(1024)}, u32[]{:S(2)}) copy-start(f32[2048]{0:T(1024)} %param.26) | copy-start | bytes 24580
  235.9 499.0 %all-gather.5.cloned.1.call-start = ((), (), s32[]{:S(2)}) async-start(), calls=%async_computation.2 | async-start | bytes 12255232 | tf_op jit(solution)/shard_map/all_gather | solution.py:92
  236.5 507.9 %all-gather.7.cloned.1.call-start = ((), (), s32[]{:S(2)}) async-start(), calls=%async_computation.3 | async-start | bytes 12255232 | tf_op jit(solution)/shard_map/all_gather | solution.py:93
  236.6 26.7 %collective-permute-start.1 = (bf16[2816,128]{1,0:T(8,128)(2,1)S(1)}, bf16[2816,128]{1,0:T(8,128)(2,1)S(1)}, u32[]{:S(2)}, u32[]{:S(2)}) collective-permute-start(bf16[2816,128]{1,0:T(8,128)(2,1)S(1)} %copy-done.8), channel_id=1, source_target_pairs={{0,2},{2,4},{4,6},{6,8},{8,10},{10,12},{12,14},{14,16},{16,18},{18... | collective-permute-start | bytes 2162696 | tf_op jit(solution)/shard_map/ppermute | solution.py:97
  264.1 24.5 %collective-permute-start.2 = (bf16[2816,128]{1,0:T(8,128)(2,1)S(1)}, bf16[2816,128]{1,0:T(8,128)(2,1)S(1)}, u32[]{:S(2)}, u32[]{:S(2)}) collective-permute-start(bf16[2816,128]{1,0:T(8,128)(2,1)S(1)} %collective-permute-done.1), channel_id=1, source_target_pairs={{0,2},{2,4},{4,6},{6,8},{8,10},{10,12},{12,14},{14,16},{16,18},{18... | collective-permute-start | bytes 2162696 | tf_op jit(solution)/shard_map/ppermute | solution.py:97
  288.6 397.8 %copy-start.12 = (bf16[2816,128]{1,0:T(8,128)(2,1)}, bf16[2816,128]{1,0:T(8,128)(2,1)S(1)}, u32[]{:S(2)}) copy-start(bf16[2816,128]{1,0:T(8,128)(2,1)S(1)} %collective-permute-done.2) | copy-start | bytes 2162692
  288.6 36.2 %collective-permute-start.3 = (bf16[2816,128]{1,0:T(8,128)(2,1)S(1)}, bf16[2816,128]{1,0:T(8,128)(2,1)S(1)}, u32[]{:S(2)}, u32[]{:S(2)}) collective-permute-start(bf16[2816,128]{1,0:T(8,128)(2,1)S(1)} %collective-permute-done.2), channel_id=1, source_target_pairs={{0,2},{2,4},{4,6},{6,8},{8,10},{10,12},{12,14},{14,16},{16,18},{18... | collective-permute-start | bytes 2162696 | tf_op jit(solution)/shard_map/ppermute | solution.py:97
  288.7 480.2 %reduce-scatter.2.cloned.1.call-start = ((), (), s32[]{:S(2)}) async-start(), calls=%async_computation.4 | async-start | bytes 2359296 | tf_op jit(solution)/shard_map/reduce_scatter | solution.py:104
  324.9 361.6 %copy-start.14 = (bf16[2816,128]{1,0:T(8,128)(2,1)}, bf16[2816,128]{1,0:T(8,128)(2,1)S(1)}, u32[]{:S(2)}) copy-start(bf16[2816,128]{1,0:T(8,128)(2,1)S(1)} %collective-permute-done.3) | copy-start | bytes 2162692
  324.9 26.7 %collective-permute-start.4 = (bf16[2816,128]{1,0:T(8,128)(2,1)S(1)}, bf16[2816,128]{1,0:T(8,128)(2,1)S(1)}, u32[]{:S(2)}, u32[]{:S(2)}) collective-permute-start(bf16[2816,128]{1,0:T(8,128)(2,1)S(1)} %collective-permute-done.3), channel_id=1, source_target_pairs={{0,2},{2,4},{4,6},{6,8},{8,10},{10,12},{12,14},{14,16},{16,18},{18... | collective-permute-start | bytes 2162696 | tf_op jit(solution)/shard_map/ppermute | solution.py:97
  352.5 37.5 %collective-permute-start.5 = (bf16[2816,128]{1,0:T(8,128)(2,1)S(1)}, bf16[2816,128]{1,0:T(8,128)(2,1)S(1)}, u32[]{:S(2)}, u32[]{:S(2)}) collective-permute-start(bf16[2816,128]{1,0:T(8,128)(2,1)S(1)} %collective-permute-done.4), channel_id=1, source_target_pairs={{0,2},{2,4},{4,6},{6,8},{8,10},{10,12},{12,14},{14,16},{16,18},{18... | collective-permute-start | bytes 2162696 | tf_op jit(solution)/shard_map/ppermute | solution.py:97
  390.8 34.3 %collective-permute-start.6 = (bf16[2816,128]{1,0:T(8,128)(2,1)S(1)}, bf16[2816,128]{1,0:T(8,128)(2,1)S(1)}, u32[]{:S(2)}, u32[]{:S(2)}) collective-permute-start(bf16[2816,128]{1,0:T(8,128)(2,1)S(1)} %collective-permute-done.5), channel_id=1, source_target_pairs={{0,2},{2,4},{4,6},{6,8},{8,10},{10,12},{12,14},{14,16},{16,18},{18... | collective-permute-start | bytes 2162696 | tf_op jit(solution)/shard_map/ppermute | solution.py:97
  426.0 36.8 %collective-permute-start.7 = (bf16[2816,128]{1,0:T(8,128)(2,1)S(1)}, bf16[2816,128]{1,0:T(8,128)(2,1)S(1)}, u32[]{:S(2)}, u32[]{:S(2)}) collective-permute-start(bf16[2816,128]{1,0:T(8,128)(2,1)S(1)} %collective-permute-done.6), channel_id=1, source_target_pairs={{0,2},{2,4},{4,6},{6,8},{8,10},{10,12},{12,14},{14,16},{16,18},{18... | collective-permute-start | bytes 2162696 | tf_op jit(solution)/shard_map/ppermute | solution.py:97
  463.6 29.2 %collective-permute-start.8 = (bf16[2816,128]{1,0:T(8,128)(2,1)S(1)}, bf16[2816,128]{1,0:T(8,128)(2,1)S(1)}, u32[]{:S(2)}, u32[]{:S(2)}) collective-permute-start(bf16[2816,128]{1,0:T(8,128)(2,1)S(1)} %collective-permute-done.7), channel_id=1, source_target_pairs={{0,2},{2,4},{4,6},{6,8},{8,10},{10,12},{12,14},{14,16},{16,18},{18... | collective-permute-start | bytes 2162696 | tf_op jit(solution)/shard_map/ppermute | solution.py:97
  493.7 25.1 %collective-permute-start.9 = (bf16[2816,128]{1,0:T(8,128)(2,1)S(1)}, bf16[2816,128]{1,0:T(8,128)(2,1)S(1)}, u32[]{:S(2)}, u32[]{:S(2)}) collective-permute-start(bf16[2816,128]{1,0:T(8,128)(2,1)S(1)} %collective-permute-done.8), channel_id=1, source_target_pairs={{0,2},{2,4},{4,6},{6,8},{8,10},{10,12},{12,14},{14,16},{16,18},{18... | collective-permute-start | bytes 2162696 | tf_op jit(solution)/shard_map/ppermute | solution.py:97
  519.6 33.7 %collective-permute-start.10 = (bf16[2816,128]{1,0:T(8,128)(2,1)S(1)}, bf16[2816,128]{1,0:T(8,128)(2,1)S(1)}, u32[]{:S(2)}, u32[]{:S(2)}) collective-permute-start(bf16[2816,128]{1,0:T(8,128)(2,1)S(1)} %collective-permute-done.9), channel_id=1, source_target_pairs={{0,2},{2,4},{4,6},{6,8},{8,10},{10,12},{12,14},{14,16},{16,18},{18... | collective-permute-start | bytes 2162696 | tf_op jit(solution)/shard_map/ppermute | solution.py:97
  554.2 23.1 %collective-permute-start.11 = (bf16[2816,128]{1,0:T(8,128)(2,1)S(1)}, bf16[2816,128]{1,0:T(8,128)(2,1)S(1)}, u32[]{:S(2)}, u32[]{:S(2)}) collective-permute-start(bf16[2816,128]{1,0:T(8,128)(2,1)S(1)} %collective-permute-done.10), channel_id=1, source_target_pairs={{0,2},{2,4},{4,6},{6,8},{8,10},{10,12},{12,14},{14,16},{16,18},{18... | collective-permute-start | bytes 2162696 | tf_op jit(solution)/shard_map/ppermute | solution.py:97
  578.2 37.2 %collective-permute-start.12 = (bf16[2816,128]{1,0:T(8,128)(2,1)S(1)}, bf16[2816,128]{1,0:T(8,128)(2,1)S(1)}, u32[]{:S(2)}, u32[]{:S(2)}) collective-permute-start(bf16[2816,128]{1,0:T(8,128)(2,1)S(1)} %collective-permute-done.11), channel_id=1, source_target_pairs={{0,2},{2,4},{4,6},{6,8},{8,10},{10,12},{12,14},{14,16},{16,18},{18... | collective-permute-start | bytes 2162696 | tf_op jit(solution)/shard_map/ppermute | solution.py:97
  616.3 33.1 %collective-permute-start.13 = (bf16[2816,128]{1,0:T(8,128)(2,1)S(1)}, bf16[2816,128]{1,0:T(8,128)(2,1)S(1)}, u32[]{:S(2)}, u32[]{:S(2)}) collective-permute-start(bf16[2816,128]{1,0:T(8,128)(2,1)S(1)} %collective-permute-done.12), channel_id=1, source_target_pairs={{0,2},{2,4},{4,6},{6,8},{8,10},{10,12},{12,14},{14,16},{16,18},{18... | collective-permute-start | bytes 2162696 | tf_op jit(solution)/shard_map/ppermute | solution.py:97
  649.4 37.0 %copy-start.34 = (bf16[2816,128]{1,0:T(8,128)(2,1)}, bf16[2816,128]{1,0:T(8,128)(2,1)S(1)}, u32[]{:S(2)}) copy-start(bf16[2816,128]{1,0:T(8,128)(2,1)S(1)} %collective-permute-done.13) | copy-start | bytes 2162692
  649.4 37.0 %collective-permute-start.14 = (bf16[2816,128]{1,0:T(8,128)(2,1)S(1)}, bf16[2816,128]{1,0:T(8,128)(2,1)}, u32[]{:S(2)}, u32[]{:S(2)}) collective-permute-start(bf16[2816,128]{1,0:T(8,128)(2,1)S(1)} %collective-permute-done.13), channel_id=1, source_target_pairs={{0,2},{2,4},{4,6},{6,8},{8,10},{10,12},{12,14},{14,16},{16,18},{18... | collective-permute-start | bytes 2162696 | tf_op jit(solution)/shard_map/ppermute | solution.py:97
  686.4 15.1 %collective-permute-start.15 = (bf16[2816,128]{1,0:T(8,128)(2,1)}, bf16[2816,128]{1,0:T(8,128)(2,1)S(1)}, u32[]{:S(2)}, u32[]{:S(2)}) collective-permute-start(bf16[2816,128]{1,0:T(8,128)(2,1)} %collective-permute-done.14), channel_id=1, source_target_pairs={{0,2},{2,4},{4,6},{6,8},{8,10},{10,12},{12,14},{14,16},{16,18},{18... | collective-permute-start | bytes 2162696 | tf_op jit(solution)/shard_map/ppermute | solution.py:97
  686.5 18.1 %copy-start.35 = (bf16[2816,128]{1,0:T(8,128)(2,1)S(1)}, bf16[2816,128]{1,0:T(8,128)(2,1)}, u32[]{:S(2)}) copy-start(bf16[2816,128]{1,0:T(8,128)(2,1)} %copy-done.34) | copy-start | bytes 2162692
  689.3 16.3 %copy-start.33 = (bf16[2816,128]{1,0:T(8,128)(2,1)S(1)}, bf16[2816,128]{1,0:T(8,128)(2,1)}, u32[]{:S(2)}) copy-start(bf16[2816,128]{1,0:T(8,128)(2,1)} %copy-done.32) | copy-start | bytes 2162692
  689.3 17.3 %copy-start.31 = (bf16[2816,128]{1,0:T(8,128)(2,1)S(1)}, bf16[2816,128]{1,0:T(8,128)(2,1)}, u32[]{:S(2)}) copy-start(bf16[2816,128]{1,0:T(8,128)(2,1)} %copy-done.30) | copy-start | bytes 2162692
  702.5 5.1 copy-start.29
  704.6 3.9 copy-start.27
  705.6 3.9 copy-start.25
  706.5 3.9 copy-start.23
  707.6 3.9 copy-start.21
  708.5 3.9 copy-start.19
  709.5 4.0 copy-start.17
  710.5 3.9 copy-start.15
  711.5 3.9 copy-start.13
  712.5 3.9 copy-start.11
  713.4 3.9 copy-start.9
  731.0 3.9 copy-start.56
  744.4 25.8 %copy-start.53 = (f32[2048]{0:T(1024)S(1)}, f32[2048]{0:T(1024)}, u32[]{:S(2)}) copy-start(f32[2048]{0:T(1024)} %param.31) | copy-start | bytes 24580
  744.4 28.2 %copy-start.1 = (bf16[16,64,64]{2,1,0:T(8,128)(2,1)S(1)}, bf16[16,64,64]{2,1,0:T(8,128)(2,1)}, u32[]{:S(2)}) copy-start(bf16[16,64,64]{2,1,0:T(8,128)(2,1)} %param.22) | copy-start | bytes 393220
  (13 other events, 11.9 us)
Sparse Core Ops, SparseCore 0:
  236.1 19.3 all-reduce.33
  763.9 4.9 reduce-scatter.1
Sparse Core Ops, SparseCore 1:
  239.2 204.6 all-gather.4
  446.4 221.9 all-gather.6
